TPU v7x, 32 devices: a whole 2x2x4 slice. The times are simulated.
32 devices in a mesh: sp: 16 (over z, y, x), tp: 2 (over core).
Axes of the slice: x: 2, y: 2, z: 4, core: 2. Of those that a mesh axis runs over, the one named last changes fastest.
Arguments:
- tokens: bfloat16 [4096, 2048], P('sp', 'tp'), may hold values from -6 to 6
- outer_gate: bfloat16 [2048, 1024], P(None, 'tp'), may hold values from -0.125 to 0.125
- inner_gate: bfloat16 [2048, 1024], P(None, 'tp'), may hold values from -0.125 to 0.125
- conv_input: bfloat16 [2048, 1024], P(None, 'tp'), may hold values from -0.125 to 0.125
- conv_taps: bfloat16 [3, 1024], P(None, 'tp'), may hold values from -3.5 to 3.5
- query_down: bfloat16 [2048, 512], P(None, 'tp'), may hold values from -0.125 to 0.125
- latent_down: bfloat16 [2048, 256], P(None, 'tp'), may hold values from -0.125 to 0.125
- rotary_down: bfloat16 [2048, 32], replicated, may hold values from -5.303301 to 5.303301
- query_gain: float32 [512], replicated, may hold values from 0.1 to 1.9
- latent_gain: float32 [256], replicated, may hold values from 0.1 to 1.9
- query_up: bfloat16 [512, 1536], P(None, 'tp'), may hold values from -0.52734375 to 0.52734375
- latent_up: bfloat16 [256, 2048], P(None, 'tp'), may hold values from -0.75 to 0.75
- conv_project: bfloat16 [1024, 2048], P('tp'), may hold values from -0.1875 to 0.1875
- attend_project: bfloat16 [1024, 2048], P('tp'), may hold values from -0.1875 to 0.1875
Outputs:
- mixed: bfloat16 [4096, 2048], P(('sp', 'tp'))
All inputs are finite; a program needn't handle non-finite values.
Results may differ from a plain program's by a relative error of at most 0.035.
Values may be sent and summed in bfloat16 or wider, within the bound.
A program may use at most 128 MiB of HBM per device.

v0:
```python
import math
import jax
import jax.numpy as jnp
from jax import lax
from jax.sharding import PartitionSpec as P

NOPE = 64
ROPE = 32
VDIM = 64
neg_fill = -1e30
rotary_base = 10000.0
norm_epsilon = 1e-06


def shifted(shard, axis, by):
    length = lax.axis_size(axis)
    pairs = [(i, i + by) for i in range(length) if 0 <= i + by < length]
    return lax.ppermute(shard, axis, pairs)


def rotate(values, positions):
    half = values.shape[-1] // 2
    inverse = rotary_base ** (-(jnp.arange(half, dtype=jnp.float32) * 2.0 / (2 * half)))
    angle = positions[:, None] * inverse[None, :]
    if values.ndim == 3:
        angle = angle[:, None, :]
    cosine = jnp.cos(angle)
    sine = jnp.sin(angle)
    first = values[..., :half]
    second = values[..., half:]
    return jnp.concatenate([first * cosine - second * sine, first * sine + second * cosine], -1)


def rms_scale(latent, gain):
    values = latent.astype(jnp.float32)
    factor = lax.rsqrt(jnp.mean(values * values, -1, keepdims=True) + norm_epsilon)
    return (values * factor * gain).astype(jnp.bfloat16)


def local(
    tokens,
    outer_gate,
    inner_gate,
    conv_input,
    conv_taps,
    query_down,
    latent_down,
    rotary_down,
    query_gain,
    latent_gain,
    query_up,
    latent_up,
    conv_project,
    attend_project,
):
    tok_rows = tokens.shape[0]
    local_heads = query_up.shape[1] // (NOPE + ROPE)
    weights = (outer_gate, inner_gate, conv_input, query_down, latent_down, rotary_down)
    piece = lax.all_gather(tokens, "tp", axis=1, tiled=True)
    outer, inner, signal, query_part, latent_part, rotary_raw = tuple(
        (jnp.dot(piece, weight, preferred_element_type=jnp.float32) for weight in weights)
    )
    query_lat, latent_lat = (
        lax.all_gather(query_part.astype(jnp.bfloat16), "tp", axis=1, tiled=True),
        lax.all_gather(latent_part.astype(jnp.bfloat16), "tp", axis=1, tiled=True),
    )
    gated = (inner * signal).astype(jnp.bfloat16)
    reach = conv_taps.shape[0] - 1
    rim = shifted(gated[tok_rows - reach :], "sp", 1)
    padded = jnp.concatenate([rim, gated], 0).astype(jnp.float32)
    taps = conv_taps.astype(jnp.float32)
    filtered = padded[0:tok_rows] * taps[0]
    for index in range(1, reach + 1):
        filtered = filtered + padded[index : index + tok_rows] * taps[index]
    conv_result = (outer * filtered).astype(jnp.bfloat16)
    seq_index = lax.axis_index("sp")
    offset = seq_index * tok_rows
    query_index = offset + jnp.arange(tok_rows, dtype=jnp.int32)
    positions = query_index.astype(jnp.float32)
    query_norm = rms_scale(query_lat, query_gain)
    latent_norm = rms_scale(latent_lat, latent_gain)
    rotary_key = rotate(rotary_raw, positions).astype(jnp.bfloat16)
    query_full = jnp.dot(query_norm, query_up, preferred_element_type=jnp.float32)
    query_full = query_full.reshape(tok_rows, local_heads, NOPE + ROPE)
    query_plain = query_full[..., :NOPE].astype(jnp.bfloat16)
    query_rot = rotate(query_full[..., NOPE:], positions).astype(jnp.bfloat16)
    scale = (NOPE + ROPE) ** (-0.5)
    query_sets = ((query_plain, query_rot, query_index),)
    set_lasts = tuple((jnp.max(members[2]) for members in query_sets))
    overall_last = set_lasts[0]

    def update(current, members, key_plain, values, rot_block, first, block):
        plain, turned, indices = members
        best, total, accum = current
        scores = jnp.einsum("qhd,khd->hqk", plain, key_plain, preferred_element_type=jnp.float32)
        scores = scores + jnp.einsum(
            "qhr,kr->hqk", turned, rot_block, preferred_element_type=jnp.float32
        )
        scores = scores * scale
        key_index = first + jnp.arange(block, dtype=jnp.int32)
        visible = key_index[None, :] <= indices[:, None]
        scores = jnp.where(visible[None], scores, neg_fill)
        new_best = jnp.maximum(best, jnp.max(scores, -1))
        factor = jnp.exp(best - new_best)
        weight = jnp.exp(scores - new_best[..., None])
        total = total * factor + jnp.sum(weight, -1)
        accum = accum * factor[..., None] + jnp.einsum(
            "hqk,khd->hqd", weight.astype(jnp.bfloat16), values, preferred_element_type=jnp.float32
        )
        return (new_best, total, accum)

    initial = tuple(
        (
            (
                jnp.full((local_heads, members[2].shape[0]), neg_fill, jnp.float32),
                jnp.zeros((local_heads, members[2].shape[0]), jnp.float32),
                jnp.zeros((local_heads, members[2].shape[0], VDIM), jnp.float32),
            )
            for members in query_sets
        )
    )
    carry = initial
    keys_latent = lax.all_gather(latent_norm, "sp", axis=0, tiled=True)
    keys_rot = lax.all_gather(rotary_key, "sp", axis=0, tiled=True)
    count = keys_latent.shape[0]
    block = math.gcd(count, 512)
    latent_blocks = keys_latent.reshape(count // block, block, keys_latent.shape[1])
    rot_blocks = keys_rot.reshape(count // block, block, keys_rot.shape[1])

    def advance(states, inputs):
        latent_block, rot_block, number = inputs
        first = number * block

        def compute(current):
            expanded = jnp.dot(latent_block, latent_up, preferred_element_type=jnp.float32)
            expanded = expanded.astype(jnp.bfloat16).reshape(block, local_heads, NOPE + VDIM)
            key_plain = expanded[..., :NOPE]
            values = expanded[..., NOPE:]
            results = []
            for members, last, state in zip(query_sets, set_lasts, current):
                results.append(
                    lax.cond(
                        first > last,
                        lambda kept: kept,
                        lambda kept, members=members: update(
                            kept, members, key_plain, values, rot_block, first, block
                        ),
                        state,
                    )
                )
            return tuple(results)

        return (lax.cond(first > overall_last, lambda current: current, compute, states), None)

    numbers = jnp.arange(count // block, dtype=jnp.int32)
    carry, unused = lax.scan(advance, carry, (latent_blocks, rot_blocks, numbers))
    states = carry
    outputs = []
    for state in states:
        best, total, accum = state
        rows = accum.shape[1]
        outputs.append(
            (accum / total[..., None])
            .transpose(1, 0, 2)
            .reshape(rows, local_heads * VDIM)
            .astype(jnp.bfloat16)
        )
    attended = outputs[0]
    return lax.psum_scatter(
        (
            jnp.dot(conv_result, conv_project, preferred_element_type=jnp.float32)
            + jnp.dot(attended, attend_project, preferred_element_type=jnp.float32)
        ).astype(jnp.bfloat16),
        "tp",
        scatter_dimension=0,
        tiled=True,
    )


def solution(mesh):
    in_specs = (
        P("sp", "tp"),
        P(None, "tp"),
        P(None, "tp"),
        P(None, "tp"),
        P(None, "tp"),
        P(None, "tp"),
        P(None, "tp"),
        P(),
        P(),
        P(),
        P(None, "tp"),
        P(None, "tp"),
        P("tp", None),
        P("tp", None),
    )
    out_specs = P(("sp", "tp"), None)
    return jax.shard_map(local, mesh=mesh, in_specs=in_specs, out_specs=out_specs, check_vma=False)
```

profile of v0, /device:TPU:0, one launch (start us, length us, event | category | flops | bytes accessed | tf_op | source)
XLA Modules:
  0.0 229.9 jit_solution(8106722850243884223)
XLA Ops:
  6.5 0.7 all-gather.3.cloned.1.call-update
  7.3 13.4 %all-gather.3.cloned.1.call-done = bf16[256,2048]{1,0:T(8,128)(2,1)} async-done(((bf16[256,1024]{1,0:T(8,128)(2,1)}), bf16[256,2048]{1,0:T(8,128)(2,1)}) %all-gather.3.cloned.1.call-update) | async-done | bytes 1048592 | tf_op jit(solution)/shard_map/all_gather | solution.py:59
  20.7 1.9 convolution_convert_fusion.2
  22.5 1.9 all_gather.16
  24.6 0.8 fusion.34
  25.4 0.7 fusion.43
  26.2 2.4 %fusion.46 = f32[256,512]{1,0:T(8,128)S(1)} fusion(bf16[256,2048]{1,0:T(8,128)(2,1)S(1)} %copy-done.2, bf16[2048,512]{1,0:T(8,128)(2,1)} %param.22), kind=kOutput, calls=%fused_computation.75 | convolution fusion | flops 536870912 | bytes 3670016 | tf_op jit(solution)/shard_map/dot_general | solution.py:61
  28.6 0.7 fusion.23
  29.4 3.8 %collective-permute-start = (bf16[2,512]{1,0:T(2,128)(2,1)S(1)}, bf16[2,512]{1,0:T(2,128)(2,1)S(1)}, u32[]{:S(2)}, u32[]{:S(2)}) collective-permute-start(bf16[2,512]{1,0:T(2,128)(2,1)S(1)} %slice.66), channel_id=1, source_target_pairs={{0,2},{2,4},{4,6},{6,8},{8,10},{10,12},{12,14},{14,16},{16,18},{18... | collective-permute-start | bytes 6152 | tf_op jit(solution)/shard_map/ppermute | solution.py:18
  33.6 2.0 all_gather.18
  36.2 40.8 %all_gather.19 = bf16[4096,32]{0,1:T(8,128)(2,1)S(1)} all-gather(bf16[256,32]{0,1:T(8,128)(2,1)S(1)} %pad_maximum_fusion.1), channel_id=1, replica_groups=mesh['sp'=16,'tp'=2] {'sp'}, dimensions={0}, use_global_device_ids=true | all-gather | bytes 278528 | tf_op jit(solution)/shard_map/all_gather | solution.py:124
  77.1 0.5 fusion.35
  77.8 0.7 copy.29
  78.5 0.9 maximum_convert_fusion
  79.4 4.7 %fusion.24 = f32[256,2048]{1,0:T(8,128)} fusion(bf16[512,2048]{1,0:T(8,128)(2,1)S(1)} %copy-done, bf16[256,2048]{1,0:T(8,128)(2,1)S(1)} %copy-done.2, bf16[2048,512]{1,0:T(8,128)(2,1)} %param.21, f32[258,512]{1,0:T(8,128)} %maximum_convert_fusion, f32[512]{0:T(512)S(1)} %bitcast.60, f32[512]{0:T(512)S(1)} %bitcast.59, f32[512]{0:T(512)S(1)} %bitcast.58), kind=kOutput, calls=%fused_computation.32 | convolution fusion | flops 1074659328 | bytes 8919040 | tf_op jit(solution)/shard_map/dot_general | solution.py:171
  84.1 3.9 %all-gather.5.cloned.1.call-done = bf16[4096,256]{1,0:T(8,128)(2,1)} async-done(((bf16[256,256]{1,0:T(8,128)(2,1)}), bf16[4096,256]{1,0:T(8,128)(2,1)}) %all-gather.5.cloned.1.call-update) | async-done | bytes 2097168 | tf_op jit(solution)/shard_map/all_gather | solution.py:123
  88.0 0.6 iota.21
  88.6 0.8 broadcast_in_dim.24
  89.5 37.1 %while.15 = (s32[]{:T(128)}, f32[8,256]{1,0:T(8,128)S(1)}, f32[8,256]{1,0:T(8,128)S(1)}, f32[8,256,64]{1,2,0:T(8,128)}, s32[8]{0:T(128)}, /*index=5*/s32[]{:T(12...) while((s32[]{:T(128)}, f32[8,256]{1,0:T(8,128)S(1)}, ...), condition=%wide.region_10.11_spmd.clone, body=%wide.region_3.10_spmd.clone.sunk | while | flops 613290752 | bytes 36222520 | solution.py:156
  89.5 1.3 dynamic_slice.39
  91.3 0.6 iota.36
  92.5 12.1 %conditional.4 = ((f32[8,256]{1,0:T(8,128)S(1)}, f32[8,256]{1,0:T(8,128)S(1)}, f32[8,256,64]{1,2,0:T(8,128)})) conditional(s32[]{:T(128)} %convert_element_type.122, (s32[]{:T(128)}, s32[]{:T(128)}, bf16[8,512,256]{2,1,0:T(8,128)(2,1)}, s32[]{:T(128)}, bf16[256,1024]{1,0:T(8,128)(2,1)}, /*index=5*/s32[]{:T(128)}, bf16[256,8,64]{0,2,1:T(8,128)(2,1)S(1)}, ...), branch_computations={%region_4.8_spmd, %region_9.9_spmd} | conditional | flops 613290752 | bytes 36204816 | solution.py:153
  92.5 1.6 convolution_convert_fusion
  94.1 1.3 broadcast_add_fusion
  96.0 8.7 %conditional = (f32[8,256]{1,0:T(8,128)S(1)}, f32[8,256]{1,0:T(8,128)S(1)}, f32[8,256,64]{1,2,0:T(8,128)}) conditional(s32[]{:T(128)} %convert_element_type.52, (s32[]{:T(128)}, s32[256]{0:T(256)}, bf16[512,1024]{1,0:T(8,128)(2,1)S(1)}, bf16[256,8,64]{0,2,1:T(8,128)(2,1)S(1)}, bf16[8,512,32]{1,2,0:T(8,128)(2,1)}, /*index=5*/s32[]{:T(128)}, ...), branch_computations={%region_5.6_spmd, %region_8.7_spmd} | conditional | flops 344330752 | bytes 34367116 | solution.py:142
  96.0 1.3 copy.22
  97.3 1.8 fusion.13
  99.3 2.0 fusion.44
  101.3 1.1 fusion.5
  102.7 1.2 fusion.9
  103.9 0.8 copy-done.4
  104.6 1.3 dynamic_slice.39
  106.5 0.6 iota.36
  107.8 1.3 dynamic_slice.39
  109.6 0.6 iota.36
  110.9 1.3 dynamic_slice.39
  112.8 0.6 iota.36
  114.0 1.3 dynamic_slice.39
  115.9 0.6 iota.36
  117.2 1.3 dynamic_slice.39
  119.0 0.6 iota.36
  120.3 1.3 dynamic_slice.39
  122.1 0.6 iota.36
  123.4 1.3 dynamic_slice.39
  125.3 0.6 iota.36
  126.5 1.1 divide_convert_fusion
  127.6 3.9 %fusion.21 = bf16[256,2048]{1,0:T(8,128)(2,1)} fusion(f32[256,2048]{1,0:T(8,128)} %fusion.24, bf16[256,512]{0,1:T(8,128)(2,1)S(1)} %bitcast.55, bf16[512,2048]{1,0:T(8,128)(2,1)} %param.33), kind=kOutput, calls=%fused_computation.26 | convolution fusion | flops 537919488 | bytes 5505024 | tf_op jit(solution)/shard_map/dot_general | solution.py:172
  131.6 91.8 %reduce-scatter.2.cloned.1.call-done = bf16[128,2048]{1,0:T(8,128)(2,1)} async-done(((bf16[256,2048]{1,0:T(8,128)(2,1)}), bf16[128,2048]{1,0:T(8,128)(2,1)}) %reduce-scatter.2.cloned.1.call-update) | async-done | bytes 524304 | tf_op jit(solution)/shard_map/reduce_scatter | solution.py:169
  (74 shorter events, 2.2 us)
Async XLA Ops:
  6.5 72.9 %copy-start = (bf16[512,2048]{1,0:T(8,128)(2,1)S(1)}, bf16[512,2048]{1,0:T(8,128)(2,1)}, u32[]{:S(2)}) copy-start(bf16[512,2048]{1,0:T(8,128)(2,1)} %param.32) | copy-start | bytes 6291460
  6.5 18.1 %copy-start.12 = (f32[256]{0:T(256)S(1)}, f32[256]{0:T(256)}, u32[]{:S(2)}) copy-start(f32[256]{0:T(256)} %param.29) | copy-start | bytes 3076
  6.5 19.6 %copy-start.10 = (bf16[3,512]{1,0:T(4,128)(2,1)S(1)}, bf16[3,512]{1,0:T(4,128)(2,1)}, u32[]{:S(2)}) copy-start(bf16[3,512]{1,0:T(4,128)(2,1)} %param.24) | copy-start | bytes 9220
  6.5 14.1 %all-gather.3.cloned.1.call-start = ((), (), s32[]{:S(2)}) async-start(), calls=%async_computation.1 | async-start | bytes 1572864 | tf_op jit(solution)/shard_map/all_gather | solution.py:59
  7.3 80.8 %all-gather.5.cloned.1.call-start = ((), (), s32[]{:S(2)}) async-start(), calls=%async_computation.2 | async-start | bytes 2228224 | tf_op jit(solution)/shard_map/all_gather | solution.py:123
  20.7 5.5 %copy-start.2 = (bf16[256,2048]{1,0:T(8,128)(2,1)S(1)}, bf16[256,2048]{1,0:T(8,128)(2,1)}, u32[]{:S(2)}) copy-start(bf16[256,2048]{1,0:T(8,128)(2,1)} %all-gather.3.cloned.1.call-done) | copy-start | bytes 3145732
  25.4 198.0 %reduce-scatter.2.cloned.1.call-start = ((), (), s32[]{:S(2)}) async-start(), calls=%async_computation.3 | async-start | bytes 1572864 | tf_op jit(solution)/shard_map/reduce_scatter | solution.py:169
  26.1 2.5 %copy-start.5 = (bf16[2048,512]{1,0:T(8,128)(2,1)S(1)}, bf16[2048,512]{1,0:T(8,128)(2,1)}, u32[]{:S(2)}) copy-start(bf16[2048,512]{1,0:T(8,128)(2,1)} %param.23) | copy-start | bytes 6291460
  28.6 4.6 %copy-start.6 = (bf16[2048,256]{1,0:T(8,128)(2,1)S(1)}, bf16[2048,256]{1,0:T(8,128)(2,1)}, u32[]{:S(2)}) copy-start(bf16[2048,256]{1,0:T(8,128)(2,1)} %param.25) | copy-start | bytes 3145732
  29.3 6.3 %copy-start.8 = (bf16[2048,32]{0,1:T(8,128)(2,1)S(1)}, bf16[2048,32]{0,1:T(8,128)(2,1)}, u32[]{:S(2)}) copy-start(bf16[2048,32]{0,1:T(8,128)(2,1)} %param.27) | copy-start | bytes 393220
  29.4 47.8 %copy-start.7 = (bf16[512,768]{1,0:T(8,128)(2,1)S(1)}, bf16[512,768]{1,0:T(8,128)(2,1)}, u32[]{:S(2)}) copy-start(bf16[512,768]{1,0:T(8,128)(2,1)} %param.30) | copy-start | bytes 2359300
  29.4 47.8 %copy-start.11 = (f32[512]{0:T(512)S(1)}, f32[512]{0:T(512)}, u32[]{:S(2)}) copy-start(f32[512]{0:T(512)} %param.28) | copy-start | bytes 6148
  29.4 49.1 %collective-permute-start = (bf16[2,512]{1,0:T(2,128)(2,1)S(1)}, bf16[2,512]{1,0:T(2,128)(2,1)S(1)}, u32[]{:S(2)}, u32[]{:S(2)}) collective-permute-start(bf16[2,512]{1,0:T(2,128)(2,1)S(1)} %slice.66), channel_id=1, source_target_pairs={{0,2},{2,4},{4,6},{6,8},{8,10},{10,12},{12,14},{14,16},{16,18},{18... | collective-permute-start | bytes 6152 | tf_op jit(solution)/shard_map/ppermute | solution.py:18
  97.3 1.8 copy-start.9
  101.3 1.2 copy-start.1
  101.3 1.3 copy-start.3
  103.8 0.8 copy-start.4
Sparse Core Ops, SparseCore 0:
  8.9 11.7 all-gather.2
  25.5 62.4 all-gather.4
  131.7 91.6 reduce-scatter.1
where the time goes:
time: 232 us; the launch traced here: 230 us
  waiting for transfers between devices  110 us (47%)
  blocking collectives  44.7 us (19%)
  matrix products  21.5 us (9%)
  local copies, waits for them, and re-layouts  19.4 us (8%)
  between operations  13.3 us (6%)
  loops' own time  11 us (5%)
  other arithmetic  6.35 us (3%)
  starting transfers between devices  3.85 us (2%)
    reduce_scatter x1, waiting for transfers between devices, local(): lax.psum_scatter((jnp.dot(conv_result, conv_project, preferred_element_ty...  91.8 us
    all_gather x1, blocking collectives, local(): keys_rot = lax.all_gather(rotary_key, 'sp', axis=0, tiled=True)  40.8 us
    all_gather x1, waiting for transfers between devices, local(): piece = lax.all_gather(tokens, 'tp', axis=1, tiled=True)  13.4 us
    dynamic_slice x8, local copies, waits for them, and re-layouts, local(): lax.scan(advance, carry, (latent_blocks, rot_blocks, numbers))  10.2 us
    another operation x1, loops' own time, local(): lax.scan(advance, carry, (latent_blocks, rot_blocks, numbers))  10 us
    dot_general x5, matrix products, local(): jnp.dot(piece, weight, preferred_element_type=jnp.float32)  5.85 us
    dot_general x1, matrix products, local(): jnp.dot(conv_result, conv_project, preferred_element_type=jnp.float32)  4.74 us
  transfers between devices with their start and end apart: 4, of which 3 were waited for; matrix products, arithmetic and copies ran while one was open for 5% of the time, Pallas kernels for 0%

commit v1 on v0

--- a/solution.py
+++ b/solution.py
@@ -53,6 +53,14 @@
     conv_project,
     attend_project,
 ):
+
+    def detail_frame(field_in, sheet, across):
+        return jnp.split(
+            lax.all_gather(jnp.concatenate([field_in, sheet], axis=1), across, axis=0, tiled=True),
+            [field_in.shape[1]],
+            axis=1,
+        )
+
     tok_rows = tokens.shape[0]
     local_heads = query_up.shape[1] // (NOPE + ROPE)
     weights = (outer_gate, inner_gate, conv_input, query_down, latent_down, rotary_down)
@@ -120,8 +128,7 @@
         )
     )
     carry = initial
-    keys_latent = lax.all_gather(latent_norm, "sp", axis=0, tiled=True)
-    keys_rot = lax.all_gather(rotary_key, "sp", axis=0, tiled=True)
+    keys_latent, keys_rot = detail_frame(latent_norm, rotary_key, "sp")
     count = keys_latent.shape[0]
     block = math.gcd(count, 512)
     latent_blocks = keys_latent.reshape(count // block, block, keys_latent.shape[1])

time: 232 us -> 246 us (1.060)
  waiting for transfers between devices: 110 us -> 158 us
  blocking collectives: 44.7 us -> 3.92 us
  local copies, waits for them, and re-layouts: 19.4 us -> 23.8 us
    all_gather x1, waiting for transfers between devices: 3.88 us -> 52.6 us  [detail_frame(): lax.all_gather(jnp.concatenate([field_in, sheet], axis=1), across, axis=0...]
    all_gather x1 -> x0, blocking collectives: 40.8 us -> none  [local(): keys_rot = lax.all_gather(rotary_key, 'sp', axis=0, tiled=True)]
    split x0 -> x3, local copies, waits for them, and re-layouts: none -> 4.3 us  [detail_frame(): jnp.split(lax.all_gather(jnp.concatenate([field_in, sheet], axis=1), acro...]
  transfers between devices with their start and end apart: 4 -> 4, of which waited for: 3 -> 3; matrix products, arithmetic and copies ran while one was open for 5% -> 4% of each run, Pallas kernels for 0% -> 0%
where the time goes in v1:
time: 246 us; the launch traced here: 244 us
  waiting for transfers between devices  158 us (64%)
  local copies, waits for them, and re-layouts  23.8 us (10%)
  matrix products  22.8 us (9%)
  between operations  13.4 us (5%)
  loops' own time  11.4 us (5%)
  other arithmetic  6.47 us (3%)
  blocking collectives  3.92 us (2%)
  starting transfers between devices  3.85 us (2%)
    reduce_scatter x1, waiting for transfers between devices, local(): lax.psum_scatter((jnp.dot(conv_result, conv_project, preferred_element_ty...  91.4 us
    all_gather x1, waiting for transfers between devices, detail_frame(): lax.all_gather(jnp.concatenate([field_in, sheet], axis=1), across, axis=0...  52.6 us
    all_gather x1, waiting for transfers between devices, local(): piece = lax.all_gather(tokens, 'tp', axis=1, tiled=True)  13.3 us
    another operation x1, loops' own time, local(): lax.scan(advance, carry, (latent_blocks, rot_blocks, numbers))  10.5 us
    dynamic_slice x8, local copies, waits for them, and re-layouts, local(): lax.scan(advance, carry, (latent_blocks, rot_blocks, numbers))  9.8 us
    dot_general x5, matrix products, local(): jnp.dot(piece, weight, preferred_element_type=jnp.float32)  7.08 us
  transfers between devices with their start and end apart: 4, of which 3 were waited for; matrix products, arithmetic and copies ran while one was open for 4% of the time, Pallas kernels for 0%

profile of v1, /device:TPU:0, one launch (start us, length us, event | category | flops | bytes accessed | tf_op | source)
XLA Modules:
  0.0 243.7 jit_solution(11248025624507622457)
XLA Ops:
  6.5 0.7 all-gather.3.cloned.1.call-update
  7.4 13.3 %all-gather.3.cloned.1.call-done = bf16[256,2048]{1,0:T(8,128)(2,1)} async-done(((bf16[256,1024]{1,0:T(8,128)(2,1)}), bf16[256,2048]{1,0:T(8,128)(2,1)}) %all-gather.3.cloned.1.call-update) | async-done | bytes 1048592 | tf_op jit(solution)/shard_map/all_gather | solution.py:67
  20.7 1.9 convolution_convert_fusion.2
  22.5 1.9 all_gather.13
  24.6 1.6 fusion.47
  26.8 0.8 pad_maximum_fusion
  27.6 0.7 fusion.43
  28.3 2.4 fusion.46
  30.8 0.7 fusion.23
  31.5 3.8 %collective-permute-start = (bf16[2,512]{1,0:T(2,128)(2,1)S(1)}, bf16[2,512]{1,0:T(2,128)(2,1)S(1)}, u32[]{:S(2)}, u32[]{:S(2)}) collective-permute-start(bf16[2,512]{1,0:T(2,128)(2,1)S(1)} %slice.66), channel_id=1, source_target_pairs={{0,2},{2,4},{4,6},{6,8},{8,10},{10,12},{12,14},{14,16},{16,18},{18... | collective-permute-start | bytes 6152 | tf_op jit(solution)/shard_map/ppermute | solution.py:18
  35.7 2.0 all_gather.15
  38.5 0.9 maximum_convert_fusion
  39.4 4.8 %fusion.24 = f32[256,2048]{1,0:T(8,128)} fusion(bf16[512,2048]{1,0:T(8,128)(2,1)S(1)} %copy-done, bf16[256,2048]{1,0:T(8,128)(2,1)S(1)} %copy-done.2, bf16[2048,512]{1,0:T(8,128)(2,1)} %param.21, f32[258,512]{1,0:T(8,128)} %maximum_convert_fusion, f32[512]{0:T(512)S(1)} %bitcast.56, f32[512]{0:T(512)S(1)} %bitcast.55, f32[512]{0:T(512)S(1)} %bitcast.54), kind=kOutput, calls=%fused_computation.32 | convolution fusion | flops 1074659328 | bytes 8919040 | tf_op jit(solution)/shard_map/dot_general | solution.py:178
  44.2 52.6 %all-gather.5.cloned.1.call-done = bf16[4096,288]{1,0:T(8,128)(2,1)} async-done(((bf16[256,288]{1,0:T(8,128)(2,1)}), bf16[4096,288]{1,0:T(8,128)(2,1)}) %all-gather.5.cloned.1.call-update) | async-done | bytes 2359312 | tf_op jit(solution)/shard_map/all_gather | solution.py:59
  96.8 1.2 slice-done
  98.0 1.0 copy.38
  99.0 3.1 %split.8 = bf16[4096,256]{1,0:T(8,128)(2,1)} slice(bf16[4096,288]{1,0:T(8,128)(2,1)} %all-gather.5.cloned.1.call-done), slice={[0:4096], [0:256]} | slice | bytes 4194304 | tf_op jit(solution)/shard_map/split | solution.py:58
  102.6 0.8 broadcast_in_dim.24
  103.4 37.2 %while.15 = (s32[]{:T(128)}, f32[8,256]{1,0:T(8,128)S(1)}, f32[8,256]{1,0:T(8,128)S(1)}, f32[8,256,64]{1,2,0:T(8,128)}, s32[8]{0:T(128)}, /*index=5*/s32[]{:T(12...) while((s32[]{:T(128)}, f32[8,256]{1,0:T(8,128)S(1)}, ...), condition=%wide.region_10.11_spmd.clone, body=%wide.region_3.10_spmd.clone.sunk | while | flops 613290752 | bytes 36222520 | solution.py:163
  103.4 1.2 dynamic_slice.39
  105.3 0.6 iota.36
  106.5 12.1 %conditional.4 = ((f32[8,256]{1,0:T(8,128)S(1)}, f32[8,256]{1,0:T(8,128)S(1)}, f32[8,256,64]{1,2,0:T(8,128)})) conditional(s32[]{:T(128)} %convert_element_type.122, (s32[]{:T(128)}, s32[]{:T(128)}, bf16[8,512,256]{2,1,0:T(8,128)(2,1)}, s32[]{:T(128)}, bf16[256,1024]{1,0:T(8,128)(2,1)}, /*index=5*/s32[]{:T(128)}, bf16[256,8,64]{0,2,1:T(8,128)(2,1)S(1)}, ...), branch_computations={%region_4.8_spmd, %region_9.9_spmd} | conditional | flops 613290752 | bytes 36204816 | solution.py:160
  106.5 1.6 convolution_convert_fusion
  108.1 1.2 broadcast_add_fusion
  110.0 8.6 %conditional = (f32[8,256]{1,0:T(8,128)S(1)}, f32[8,256]{1,0:T(8,128)S(1)}, f32[8,256,64]{1,2,0:T(8,128)}) conditional(s32[]{:T(128)} %convert_element_type.52, (s32[]{:T(128)}, s32[256]{0:T(256)}, bf16[512,1024]{1,0:T(8,128)(2,1)S(1)}, bf16[256,8,64]{0,2,1:T(8,128)(2,1)S(1)}, bf16[8,512,32]{1,2,0:T(8,128)(2,1)}, /*index=5*/s32[]{:T(128)}, ...), branch_computations={%region_5.6_spmd, %region_8.7_spmd} | conditional | flops 344330752 | bytes 34367116 | solution.py:149
  110.0 1.3 copy.34
  111.3 1.8 fusion.13
  113.3 2.0 fusion.44
  115.3 1.1 fusion.5
  116.6 1.2 fusion.9
  117.9 0.8 copy-done.4
  118.6 1.2 dynamic_slice.39
  120.5 0.6 iota.36
  121.8 1.2 dynamic_slice.39
  123.7 0.6 iota.36
  124.9 1.2 dynamic_slice.39
  126.8 0.6 iota.36
  128.1 1.2 dynamic_slice.39
  130.0 0.6 iota.36
  131.2 1.2 dynamic_slice.39
  133.1 0.6 iota.36
  134.4 1.2 dynamic_slice.39
  136.2 0.6 iota.36
  137.5 1.2 dynamic_slice.39
  139.4 0.6 iota.36
  140.7 1.1 divide_convert_fusion
  141.8 3.9 %fusion.21 = bf16[256,2048]{1,0:T(8,128)(2,1)} fusion(f32[256,2048]{1,0:T(8,128)} %fusion.24, bf16[256,512]{0,1:T(8,128)(2,1)S(1)} %bitcast.53, bf16[512,2048]{1,0:T(8,128)(2,1)} %param.33), kind=kOutput, calls=%fused_computation.26 | convolution fusion | flops 537919488 | bytes 5505024 | tf_op jit(solution)/shard_map/dot_general | solution.py:179
  145.7 91.4 %reduce-scatter.2.cloned.1.call-done = bf16[128,2048]{1,0:T(8,128)(2,1)} async-done(((bf16[256,2048]{1,0:T(8,128)(2,1)}), bf16[128,2048]{1,0:T(8,128)(2,1)}) %reduce-scatter.2.cloned.1.call-update) | async-done | bytes 524304 | tf_op jit(solution)/shard_map/reduce_scatter | solution.py:176
  (78 shorter events, 3.1 us)
Async XLA Ops:
  6.5 32.9 %copy-start = (bf16[512,2048]{1,0:T(8,128)(2,1)S(1)}, bf16[512,2048]{1,0:T(8,128)(2,1)}, u32[]{:S(2)}) copy-start(bf16[512,2048]{1,0:T(8,128)(2,1)} %param.32) | copy-start | bytes 6291460
  6.5 18.1 %copy-start.8 = (bf16[2048,32]{0,1:T(8,128)(2,1)S(1)}, bf16[2048,32]{0,1:T(8,128)(2,1)}, u32[]{:S(2)}) copy-start(bf16[2048,32]{0,1:T(8,128)(2,1)} %param.27) | copy-start | bytes 393220
  6.5 20.1 %copy-start.12 = (f32[256]{0:T(256)S(1)}, f32[256]{0:T(256)}, u32[]{:S(2)}) copy-start(f32[256]{0:T(256)} %param.29) | copy-start | bytes 3076
  6.5 14.1 %all-gather.3.cloned.1.call-start = ((), (), s32[]{:S(2)}) async-start(), calls=%async_computation.1 | async-start | bytes 1572864 | tf_op jit(solution)/shard_map/all_gather | solution.py:67
  7.3 89.5 %all-gather.5.cloned.1.call-start = ((), (), s32[]{:S(2)}) async-start(), calls=%async_computation.2 | async-start | bytes 3342336 | tf_op jit(solution)/shard_map/all_gather | solution.py:59
  7.3 20.9 %copy-start.10 = (bf16[3,512]{1,0:T(4,128)(2,1)S(1)}, bf16[3,512]{1,0:T(4,128)(2,1)}, u32[]{:S(2)}) copy-start(bf16[3,512]{1,0:T(4,128)(2,1)} %param.24) | copy-start | bytes 9220
  20.7 7.6 %copy-start.2 = (bf16[256,2048]{1,0:T(8,128)(2,1)S(1)}, bf16[256,2048]{1,0:T(8,128)(2,1)}, u32[]{:S(2)}) copy-start(bf16[256,2048]{1,0:T(8,128)(2,1)} %all-gather.3.cloned.1.call-done) | copy-start | bytes 3145732
  27.6 209.6 %reduce-scatter.2.cloned.1.call-start = ((), (), s32[]{:S(2)}) async-start(), calls=%async_computation.3 | async-start | bytes 1572864 | tf_op jit(solution)/shard_map/reduce_scatter | solution.py:176
  28.3 2.5 %copy-start.5 = (bf16[2048,512]{1,0:T(8,128)(2,1)S(1)}, bf16[2048,512]{1,0:T(8,128)(2,1)}, u32[]{:S(2)}) copy-start(bf16[2048,512]{1,0:T(8,128)(2,1)} %param.23) | copy-start | bytes 6291460
  30.8 4.5 %copy-start.6 = (bf16[2048,256]{1,0:T(8,128)(2,1)S(1)}, bf16[2048,256]{1,0:T(8,128)(2,1)}, u32[]{:S(2)}) copy-start(bf16[2048,256]{1,0:T(8,128)(2,1)} %param.25) | copy-start | bytes 3145732
  31.5 6.4 %copy-start.7 = (bf16[512,768]{1,0:T(8,128)(2,1)S(1)}, bf16[512,768]{1,0:T(8,128)(2,1)}, u32[]{:S(2)}) copy-start(bf16[512,768]{1,0:T(8,128)(2,1)} %param.30) | copy-start | bytes 2359300
  31.5 6.4 %copy-start.11 = (f32[512]{0:T(512)S(1)}, f32[512]{0:T(512)}, u32[]{:S(2)}) copy-start(f32[512]{0:T(512)} %param.28) | copy-start | bytes 6148
  31.5 7.0 %collective-permute-start = (bf16[2,512]{1,0:T(2,128)(2,1)S(1)}, bf16[2,512]{1,0:T(2,128)(2,1)S(1)}, u32[]{:S(2)}, u32[]{:S(2)}) collective-permute-start(bf16[2,512]{1,0:T(2,128)(2,1)S(1)} %slice.66), channel_id=1, source_target_pairs={{0,2},{2,4},{4,6},{6,8},{8,10},{10,12},{12,14},{14,16},{16,18},{18... | collective-permute-start | bytes 6152 | tf_op jit(solution)/shard_map/ppermute | solution.py:18
  96.8 1.2 slice-start
  111.3 1.8 copy-start.9
  115.3 1.2 copy-start.1
  115.3 1.3 copy-start.3
  117.8 0.8 copy-start.4
Sparse Core Ops, SparseCore 0:
  8.9 11.7 all-gather.2
  27.7 69.0 all-gather.4
  145.8 91.2 reduce-scatter.1
